TPU v7x, 32 devices: a whole 2x2x4 slice. The times are simulated.
32 devices in a mesh: fs: 8 (over z, x), tp: 4 (over y, core).
Axes of the slice: x: 2, y: 2, z: 4, core: 2. Of those that a mesh axis runs over, the one named last changes fastest.
Arguments:
- tokens: bfloat16 [4096, 2048], P(('fs', 'tp')), may hold values from -6 to 6
- gate_weight: bfloat16 [5632, 2048], P('tp', 'fs'), may hold values from -0.125 to 0.125
- up_weight: bfloat16 [5632, 2048], P('tp', 'fs'), may hold values from -0.125 to 0.125
- down_weight: bfloat16 [5632, 2048], P('tp', 'fs'), may hold values from -0.078125 to 0.078125
- out_grad: bfloat16 [4096, 2048], P(('fs', 'tp')), may hold values from -6 to 6
Outputs:
- grad_tokens: bfloat16 [4096, 2048], P(('fs', 'tp'))
- grad_gate: float32 [5632, 2048], P('tp', 'fs')
- grad_up: float32 [5632, 2048], P('tp', 'fs')
- grad_down: float32 [5632, 2048], P('tp', 'fs')
- gate_rows: float32 [5632], P('tp')
- up_rows: float32 [5632], P('tp')
- down_rows: float32 [5632], P('tp')
All inputs are finite; a program needn't handle non-finite values.
Results may differ from a plain program's by a relative error of at most 0.014.
Values may be sent and summed in bfloat16 or wider, within the bound.
A program may use at most 128 MiB of HBM per device.

v0:
```python
import math
import jax
import jax.numpy as jnp
from jax import lax
from jax.sharding import PartitionSpec as P


def body(tokens, gate_weight, up_weight, down_weight, out_grad):
    inputs, cotangent = (
        lax.all_gather(tokens, "tp", axis=0, tiled=True),
        lax.all_gather(out_grad, "tp", axis=0, tiled=True),
    )
    w_gate, w_up, w_down = (
        lax.all_gather(gate_weight, "fs", axis=1, tiled=True),
        lax.all_gather(up_weight, "fs", axis=1, tiled=True),
        lax.all_gather(down_weight, "fs", axis=1, tiled=True),
    )
    inner = (((1,), (1,)), ((), ()))
    gate = lax.dot_general(inputs, w_gate, inner, preferred_element_type=jnp.float32)
    up = lax.dot_general(inputs, w_up, inner, preferred_element_type=jnp.float32)
    dhidden = lax.dot_general(cotangent, w_down, inner, preferred_element_type=jnp.float32)
    sig = jax.nn.sigmoid(gate)
    silu = gate * sig
    act = (silu * up).astype(jnp.bfloat16)
    dgate = (dhidden * up * sig * (1.0 + gate * (1.0 - sig))).astype(jnp.bfloat16)
    dup = (dhidden * silu).astype(jnp.bfloat16)
    term = jnp.dot(dgate, w_gate, preferred_element_type=jnp.float32)
    grad_tokens = lax.psum_scatter(
        (term + jnp.dot(dup, w_up, preferred_element_type=jnp.float32)).astype(jnp.bfloat16),
        "tp",
        scatter_dimension=0,
        tiled=True,
    )
    factor = 1.0 / math.sqrt(inputs.shape[0] * lax.axis_size("fs"))
    outer = (((0,), (0,)), ((), ()))
    width = gate_weight.shape[1] * lax.axis_size("fs")
    part_gate = lax.dot_general(dgate, inputs, outer, preferred_element_type=jnp.float32) * factor
    part_up = lax.dot_general(dup, inputs, outer, preferred_element_type=jnp.float32) * factor
    part_down = lax.dot_general(act, cotangent, outer, preferred_element_type=jnp.float32) * factor
    grad_gate, grad_up, grad_down = (
        lax.psum_scatter(
            part_gate.astype(jnp.bfloat16), "fs", scatter_dimension=1, tiled=True
        ).astype(jnp.float32),
        lax.psum_scatter(
            part_up.astype(jnp.bfloat16), "fs", scatter_dimension=1, tiled=True
        ).astype(jnp.float32),
        lax.psum_scatter(
            part_down.astype(jnp.bfloat16), "fs", scatter_dimension=1, tiled=True
        ).astype(jnp.float32),
    )
    sums = lax.psum(
        (
            jnp.sum(grad_gate * grad_gate, axis=1),
            jnp.sum(grad_up * grad_up, axis=1),
            jnp.sum(grad_down * grad_down, axis=1),
        ),
        "fs",
    )
    gate_rows, up_rows, down_rows = (sums[0] / width, sums[1] / width, sums[2] / width)
    return (grad_tokens, grad_gate, grad_up, grad_down, gate_rows, up_rows, down_rows)


def solution(mesh):
    return jax.shard_map(
        body,
        mesh=mesh,
        in_specs=(
            P(("fs", "tp"), None),
            P("tp", "fs"),
            P("tp", "fs"),
            P("tp", "fs"),
            P(("fs", "tp"), None),
        ),
        out_specs=(
            P(("fs", "tp"), None),
            P("tp", "fs"),
            P("tp", "fs"),
            P("tp", "fs"),
            P("tp"),
            P("tp"),
            P("tp"),
        ),
        check_vma=False,
    )
```

profile of v0, /device:TPU:0, one launch (start us, length us, event | category | flops | bytes accessed | tf_op | source)
XLA Modules:
  0.0 727.2 jit_solution(359217630501200977)
XLA Ops:
  7.2 0.7 all-gather.10.cloned.1.call-update
  7.9 0.7 all-gather.12.cloned.1.call-update
  8.7 0.7 all-gather.14.cloned.1.call-update
  9.4 0.5 all-gather.6.cloned.1.call-update
  10.0 0.5 all-gather.8.cloned.1.call-update
  10.5 0.0 reduce-scatter.11.cloned.1.call-start
  10.6 24.3 %all-gather.10.cloned.1.call-done = bf16[512,2048]{1,0:T(8,128)(2,1)} async-done(((bf16[128,2048]{1,0:T(8,128)(2,1)}), bf16[512,2048]{1,0:T(8,128)(2,1)}) %all-gather.10.cloned.1.call-update) | async-done | bytes 2097168 | tf_op jit(solution)/shard_map/all_gather | solution.py:10
  34.9 95.2 %all-gather.12.cloned.1.call-done = bf16[1408,2048]{1,0:T(8,128)(2,1)} async-done(((bf16[1408,256]{1,0:T(8,128)(2,1)}), bf16[1408,2048]{1,0:T(8,128)(2,1)}) %all-gather.12.cloned.1.call-update) | async-done | bytes 5767184 | tf_op jit(solution)/shard_map/all_gather | solution.py:15
  130.1 8.3 %fusion.3 = f32[512,1408]{1,0:T(8,128)} fusion(bf16[512,2048]{1,0:T(8,128)(2,1)} %all-gather.10.cloned.1.call-done, bf16[1408,2048]{1,0:T(8,128)(2,1)} %all-gather.12.cloned.1.call-done), kind=kOutput, calls=%fused_computation.16 | convolution fusion | flops 2952790016 | bytes 10747904 | tf_op jit(solution)/shard_map/dot_general | solution.py:20
  138.4 85.1 %all-gather.14.cloned.1.call-done = bf16[1408,2048]{1,0:T(8,128)(2,1)} async-done(((bf16[1408,256]{1,0:T(8,128)(2,1)}), bf16[1408,2048]{1,0:T(8,128)(2,1)}) %all-gather.14.cloned.1.call-update) | async-done | bytes 5767184 | tf_op jit(solution)/shard_map/all_gather | solution.py:14
  223.5 7.6 %fusion.4 = f32[512,1408]{1,0:T(8,128)} fusion(bf16[512,2048]{1,0:T(8,128)(2,1)S(1)} %copy-done, bf16[1408,2048]{1,0:T(8,128)(2,1)} %all-gather.14.cloned.1.call-done), kind=kOutput, calls=%fused_computation.17 | convolution fusion | flops 2952790016 | bytes 10747904 | tf_op jit(solution)/shard_map/dot_general | solution.py:19
  231.1 14.6 %all-gather.6.cloned.1.call-done = bf16[512,2048]{1,0:T(8,128)(2,1)} async-done(((bf16[128,2048]{1,0:T(8,128)(2,1)}), bf16[512,2048]{1,0:T(8,128)(2,1)}) %all-gather.6.cloned.1.call-update) | async-done | bytes 2097168 | tf_op jit(solution)/shard_map/all_gather | solution.py:11
  245.7 9.1 %multiply_convert_fusion = bf16[1408,2048]{1,0:T(8,128)(2,1)} fusion(bf16[512,2048]{1,0:T(8,128)(2,1)} %all-gather.6.cloned.1.call-done, f32[512,1408]{1,0:T(8,128)} %fusion.3, f32[512,1408]{1,0:T(8,128)} %fusion.4), kind=kOutput, calls=%fused_computation | convolution fusion | flops 2962882560 | bytes 13631488 | tf_op jit(solution)/shard_map/dot_general | solution.py:39
  254.7 0.2 reduce-scatter.9.cloned.1.call-start
  255.0 85.7 %all-gather.8.cloned.1.call-done = bf16[1408,2048]{1,0:T(8,128)(2,1)} async-done(((bf16[1408,256]{1,0:T(8,128)(2,1)}), bf16[1408,2048]{1,0:T(8,128)(2,1)}) %all-gather.8.cloned.1.call-update) | async-done | bytes 5767184 | tf_op jit(solution)/shard_map/all_gather | solution.py:16
  340.7 10.2 %multiply_convert_fusion.4 = (bf16[512,1408]{1,0:T(8,128)(2,1)S(1)}, bf16[512,1408]{1,0:T(8,128)(2,1)}) fusion(f32[512,1408]{1,0:T(8,128)} %fusion.4, f32[512,1408]{1,0:T(8,128)} %fusion.3, bf16[512,2048]{1,0:T(8,128)(2,1)} %all-gather.6.cloned.1.call-done, bf16[1408,2048]{1,0:T(8,128)(2,1)} %all-gather.8.cloned.1.call-done), kind=kOutput, calls=%fused_computation.5 | convolution fusion | flops 2962161664 | bytes 16515072 | tf_op jit(solution)/shard_map/dot_general | solution.py:21
  350.9 5.0 multiply_convert_fusion.1
  355.9 0.0 reduce-scatter.7.cloned.1.call-start
  355.9 6.5 multiply_convert_fusion.2
  362.4 0.0 reduce-scatter.5.cloned.1.call-start
  362.5 1.3 copy-done.1
  363.8 5.4 fusion.5
  369.2 7.4 %add_convert_fusion = bf16[512,2048]{1,0:T(8,128)(2,1)} fusion(f32[512,2048]{1,0:T(8,128)S(1)} %fusion.5, bf16[512,1408]{1,0:T(8,128)(2,1)S(1)} %get-tuple-element.16, bf16[1408,2048]{1,0:T(8,128)(2,1)} %all-gather.12.cloned.1.call-done), kind=kOutput, calls=%fused_computation.3 | convolution fusion | flops 2954887168 | bytes 13500416 | tf_op jit(solution)/shard_map/dot_general | solution.py:29
  376.6 76.8 %reduce-scatter.11.cloned.1.call-done = bf16[1408,256]{1,0:T(8,128)(2,1)} async-done(((bf16[1408,2048]{1,0:T(8,128)(2,1)}), bf16[1408,256]{1,0:T(8,128)(2,1)}) %reduce-scatter.11.cloned.1.call-update) | async-done | bytes 720912 | tf_op jit(solution)/shard_map/reduce_scatter | solution.py:47
  453.5 2.3 multiply_reduce_fusion
  455.8 111.8 %reduce-scatter.9.cloned.1.call-done = bf16[1408,256]{1,0:T(8,128)(2,1)} async-done(((bf16[1408,2048]{1,0:T(8,128)(2,1)}), bf16[1408,256]{1,0:T(8,128)(2,1)}) %reduce-scatter.9.cloned.1.call-update) | async-done | bytes 720912 | tf_op jit(solution)/shard_map/reduce_scatter | solution.py:44
  567.6 2.3 multiply_reduce_fusion.1
  569.9 111.8 %reduce-scatter.7.cloned.1.call-done = bf16[1408,256]{1,0:T(8,128)(2,1)} async-done(((bf16[1408,2048]{1,0:T(8,128)(2,1)}), bf16[1408,256]{1,0:T(8,128)(2,1)}) %reduce-scatter.7.cloned.1.call-update) | async-done | bytes 720912 | tf_op jit(solution)/shard_map/reduce_scatter | solution.py:41
  681.7 2.3 multiply_reduce_fusion.2
  684.0 35.5 %all-reduce = (f32[1408]{0:T(1024)S(1)}, f32[1408]{0:T(1024)S(1)}, f32[1408]{0:T(1024)S(1)}) all-reduce(f32[1408]{0:T(1024)S(1)} %get-tuple-element.14, f32[1408]{0:T(1024)S(1)} %get-tuple-element.12, f32[1408]{0:T(1024)S(1)} %get-tuple-element.10), channel_id=1, replica_groups=mesh['fs'=8,'tp'=4] {'fs'}, use_global_device_ids=true, to_apply=%region_5.0 | all-reduce | flops 4224 | bytes 33792 | tf_op jit(solution)/shard_map/psum | solution.py:51
  719.5 0.6 broadcast_multiply_fusion.2
  720.1 0.6 broadcast_multiply_fusion
  (13 shorter events, 0.3 us)
Async XLA Ops:
  7.2 27.7 %all-gather.10.cloned.1.call-start = ((), (), s32[]{:S(2)}) async-start(), calls=%async_computation.6 | async-start | bytes 2621440 | tf_op jit(solution)/shard_map/all_gather | solution.py:10
  7.9 122.2 %all-gather.12.cloned.1.call-start = ((), (), s32[]{:S(2)}) async-start(), calls=%async_computation.7 | async-start | bytes 6488064 | tf_op jit(solution)/shard_map/all_gather | solution.py:15
  8.6 214.8 %all-gather.14.cloned.1.call-start = ((), (), s32[]{:S(2)}) async-start(), calls=%async_computation.8 | async-start | bytes 6488064 | tf_op jit(solution)/shard_map/all_gather | solution.py:14
  9.4 236.3 %all-gather.6.cloned.1.call-start = ((), (), s32[]{:S(2)}) async-start(), calls=%async_computation.4 | async-start | bytes 2621440 | tf_op jit(solution)/shard_map/all_gather | solution.py:11
  10.0 330.7 %all-gather.8.cloned.1.call-start = ((), (), s32[]{:S(2)}) async-start(), calls=%async_computation.5 | async-start | bytes 6488064 | tf_op jit(solution)/shard_map/all_gather | solution.py:16
  10.5 442.9 %reduce-scatter.11.cloned.1.call-start = ((), (), s32[]{:S(2)}) async-start(), calls=%async_computation.12 | async-start | bytes 6488064 | tf_op jit(solution)/shard_map/reduce_scatter | solution.py:47
  34.9 188.6 %copy-start = (bf16[512,2048]{1,0:T(8,128)(2,1)S(1)}, bf16[512,2048]{1,0:T(8,128)(2,1)}, u32[]{:S(2)}) copy-start(bf16[512,2048]{1,0:T(8,128)(2,1)} %all-gather.10.cloned.1.call-done) | copy-start | bytes 6291460
  254.7 312.8 %reduce-scatter.9.cloned.1.call-start = ((), (), s32[]{:S(2)}) async-start(), calls=%async_computation.11 | async-start | bytes 6488064 | tf_op jit(solution)/shard_map/reduce_scatter | solution.py:44
  355.9 325.8 %reduce-scatter.7.cloned.1.call-start = ((), (), s32[]{:S(2)}) async-start(), calls=%async_computation.10 | async-start | bytes 6488064 | tf_op jit(solution)/shard_map/reduce_scatter | solution.py:41
  362.4 1.4 copy-start.1
  362.4 358.3 %reduce-scatter.5.cloned.1.call-start = ((), (), s32[]{:S(2)}) async-start(), calls=%async_computation.9 | async-start | bytes 2621440 | tf_op jit(solution)/shard_map/reduce_scatter | solution.py:28
Sparse Core Ops, SparseCore 0:
  9.5 25.2 all-gather.9
  36.9 93.1 all-gather.11
  132.1 91.3 all-gather.13
  224.9 20.7 all-gather.5
  247.5 93.1 all-gather.7
  344.2 109.1 reduce-scatter.10
  457.1 110.3 reduce-scatter.8
  571.2 110.3 reduce-scatter.6
  684.8 30.5 reduce-scatter.4
where the time goes:
time: 728 us; the launch traced here: 727 us
  waiting for transfers between devices  608 us (84%)
  matrix products  59.5 us (8%)
  blocking collectives  35.5 us (5%)
  between operations  13.9 us (2%)
  other arithmetic  8.24 us (1%)
    reduce_scatter x1, waiting for transfers between devices, body(): lax.psum_scatter(part_up.astype(jnp.bfloat16), 'fs', scatter_dimension=1,...  112 us
    reduce_scatter x1, waiting for transfers between devices, body(): lax.psum_scatter(part_gate.astype(jnp.bfloat16), 'fs', scatter_dimension=...  112 us
    all_gather x1, waiting for transfers between devices, body(): lax.all_gather(up_weight, 'fs', axis=1, tiled=True)  95.2 us
    all_gather x1, waiting for transfers between devices, body(): lax.all_gather(down_weight, 'fs', axis=1, tiled=True)  85.7 us
    all_gather x1, waiting for transfers between devices, body(): lax.all_gather(gate_weight, 'fs', axis=1, tiled=True)  85.1 us
    reduce_scatter x1, waiting for transfers between devices, body(): lax.psum_scatter(part_down.astype(jnp.bfloat16), 'fs', scatter_dimension=...  76.8 us
    psum x1, blocking collectives, body(): lax.psum((jnp.sum(grad_gate * grad_gate, axis=1), jnp.sum(grad_up * grad_...  35.5 us
    all_gather x1, waiting for transfers between devices, body(): lax.all_gather(tokens, 'tp', axis=0, tiled=True)  24.3 us
  transfers between devices with their start and end apart: 9, of which 8 were waited for; matrix products, arithmetic and copies ran while one was open for 9% of the time, Pallas kernels for 0%

commit v1 on v0

--- a/solution.py
+++ b/solution.py
@@ -1,8 +1,46 @@
+import functools
 import math
 import jax
 import jax.numpy as jnp
 from jax import lax
 from jax.sharding import PartitionSpec as P
+
+
+def trails_map(obj, pos_dim):
+    mid_arr, n_now, w_next = (lax.psum(1, axis_name="fs"), lax.axis_index("fs"), obj.shape[pos_dim])
+    steps_seen = []
+    for i, dd in enumerate(obj.shape):
+        steps_seen.append(dd * mid_arr if i == pos_dim else dd)
+    built = lax.dynamic_update_slice_in_dim(
+        jnp.zeros(steps_seen, obj.dtype), obj, n_now * w_next, axis=pos_dim
+    )
+    lower = answer = obj
+    w = 1
+    while w < mid_arr // 2 + 1:
+        pages = []
+        i = 0
+        while i < mid_arr:
+            pages.append((i, (i + 1) % mid_arr))
+            i += 1
+        lower = lax.ppermute(lower, axis_name="fs", perm=pages)
+        built = lax.dynamic_update_slice_in_dim(
+            built, lower, (n_now - w) % mid_arr * w_next, axis=pos_dim
+        )
+        if 2 * w < mid_arr:
+            line_up = []
+            i = 0
+            while i < mid_arr:
+                line_up.append((i, (i - 1) % mid_arr))
+                i += 1
+            answer = lax.ppermute(answer, "fs", perm=line_up)
+            built = lax.dynamic_update_slice_in_dim(
+                built, answer, (n_now + w) % mid_arr * w_next, axis=pos_dim
+            )
+        w = w + 1
+    return built
+
+
+tails_process = functools.partial(trails_map, pos_dim=1)
 
 
 def body(tokens, gate_weight, up_weight, down_weight, out_grad):
@@ -12,7 +50,7 @@
     )
     w_gate, w_up, w_down = (
         lax.all_gather(gate_weight, "fs", axis=1, tiled=True),
-        lax.all_gather(up_weight, "fs", axis=1, tiled=True),
+        tails_process(up_weight),
         lax.all_gather(down_weight, "fs", axis=1, tiled=True),
     )
     inner = (((1,), (1,)), ((), ()))

time: 728 us -> 702 us (0.964)
  waiting for transfers between devices: 608 us -> 553 us
  starting transfers between devices: 0.53 us -> 20 us
  local copies, waits for them, and re-layouts: 1.29 us -> 14.9 us
    ppermute x0 -> x7, waiting for transfers between devices: none -> 120 us  [the longest x4 120 us: trails_map(): lower = lax.ppermute(lower, axis_name='fs', perm=pages)]
    all_gather x1 -> x0, waiting for transfers between devices: 95.2 us -> none  [body(): lax.all_gather(up_weight, 'fs', axis=1, tiled=True)]
    all_gather x1, waiting for transfers between devices: 85.1 us -> 17 us  [body(): lax.all_gather(gate_weight, 'fs', axis=1, tiled=True)]
    reduce_scatter x1, waiting for transfers between devices: 76.8 us -> 112 us  [body(): lax.psum_scatter(part_down.astype(jnp.bfloat16), 'fs', scatter_dimension=...]
    reduce_scatter x1, waiting for transfers between devices: 112 us -> 80.2 us  [body(): lax.psum_scatter(part_gate.astype(jnp.bfloat16), 'fs', scatter_dimension=...]
    all_gather x1, waiting for transfers between devices: 24.3 us -> 0.01 us  [body(): lax.all_gather(tokens, 'tp', axis=0, tiled=True)]
    ppermute x0 -> x7, starting transfers between devices: none -> 19.5 us  [the longest x4 10.4 us: trails_map(): lower = lax.ppermute(lower, axis_name='fs', perm=pages)]
    all_gather x1, waiting for transfers between devices: 85.7 us -> 95.1 us  [body(): lax.all_gather(down_weight, 'fs', axis=1, tiled=True)]
  transfers between devices with their start and end apart: 9 -> 15, of which waited for: 8 -> 11; matrix products, arithmetic and copies ran while one was open for 9% -> 9% of each run, Pallas kernels for 0% -> 0%
where the time goes in v1:
time: 702 us
  waiting for transfers between devices  553 us (79%)
  matrix products  56 us (8%)
  blocking collectives  35.5 us (5%)
  starting transfers between devices  20 us (3%)
  local copies, waits for them, and re-layouts  14.9 us (2%)
  between operations  14.2 us (2%)
  other arithmetic  8.24 us (1%)
    ppermute x4, waiting for transfers between devices, trails_map(): lower = lax.ppermute(lower, axis_name='fs', perm=pages)  120 us
    reduce_scatter x1, waiting for transfers between devices, body(): lax.psum_scatter(part_down.astype(jnp.bfloat16), 'fs', scatter_dimension=...  112 us
    reduce_scatter x1, waiting for transfers between devices, body(): lax.psum_scatter(part_up.astype(jnp.bfloat16), 'fs', scatter_dimension=1,...  112 us
    all_gather x1, waiting for transfers between devices, body(): lax.all_gather(down_weight, 'fs', axis=1, tiled=True)  95.1 us
    reduce_scatter x1, waiting for transfers between devices, body(): lax.psum_scatter(part_gate.astype(jnp.bfloat16), 'fs', scatter_dimension=...  80.2 us
    psum x1, blocking collectives, body(): lax.psum((jnp.sum(grad_gate * grad_gate, axis=1), jnp.sum(grad_up * grad_...  35.5 us
    all_gather x1, waiting for transfers between devices, body(): lax.all_gather(gate_weight, 'fs', axis=1, tiled=True)  17 us
    all_gather x1, waiting for transfers between devices, body(): lax.all_gather(out_grad, 'tp', axis=0, tiled=True)  14.6 us
  transfers between devices with their start and end apart: 15, of which 11 were waited for; matrix products, arithmetic and copies ran while one was open for 9% of the time, Pallas kernels for 0%

profile of v1, /device:TPU:0, one launch (start us, length us, event | category | flops | bytes accessed | tf_op | source)
XLA Modules:
  0.0 702.0 jit_solution(4587406221404183118)
XLA Ops:
  10.0 3.0 collective-permute-start
  13.0 3.1 collective-permute-start.1
  16.1 28.1 %collective-permute-done = bf16[1408,256]{1,0:T(8,128)(2,1)S(1)} collective-permute-done((bf16[1408,256]{1,0:T(8,128)(2,1)}, bf16[1408,256]{1,0:T(8,128)(2,1)S(1)}, u32[]{:S(2)}, u32[]{:S(2)}) %collective-permute-start) | collective-permute-done | bytes 720928 | tf_op jit(solution)/shard_map/ppermute | solution.py:25
  44.2 2.4 collective-permute-start.2
  46.6 3.1 collective-permute-start.3
  49.7 3.2 broadcast_in_dim.3
  53.8 30.4 %collective-permute-done.2 = bf16[1408,256]{1,0:T(8,128)(2,1)S(1)} collective-permute-done((bf16[1408,256]{1,0:T(8,128)(2,1)S(1)}, bf16[1408,256]{1,0:T(8,128)(2,1)S(1)}, u32[]{:S(2)}, u32[]{:S(2)}) %collective-permute-start.2) | collective-permute-done | bytes 720928 | tf_op jit(solution)/shard_map/ppermute | solution.py:25
  84.2 2.5 collective-permute-start.4
  88.6 3.0 collective-permute-start.5
  92.6 33.2 %collective-permute-done.4 = bf16[1408,256]{1,0:T(8,128)(2,1)S(1)} collective-permute-done((bf16[1408,256]{1,0:T(8,128)(2,1)S(1)}, bf16[1408,256]{1,0:T(8,128)(2,1)S(1)}, u32[]{:S(2)}, u32[]{:S(2)}) %collective-permute-start.4) | collective-permute-done | bytes 720928 | tf_op jit(solution)/shard_map/ppermute | solution.py:25
  125.9 2.5 collective-permute-start.6
  132.0 27.9 %collective-permute-done.6 = bf16[1408,256]{1,0:T(8,128)(2,1)S(1)} collective-permute-done((bf16[1408,256]{1,0:T(8,128)(2,1)S(1)}, bf16[1408,256]{1,0:T(8,128)(2,1)S(1)}, u32[]{:S(2)}, u32[]{:S(2)}) %collective-permute-start.6) | collective-permute-done | bytes 720928 | tf_op jit(solution)/shard_map/ppermute | solution.py:25
  160.8 8.5 %convolution_bitcast_fusion = f32[512,1408]{1,0:T(8,128)} fusion(bf16[1408,2048]{1,0:T(8,128)(2,1)} %constant_dynamic-update-slice_fusion, bf16[512,2048]{1,0:T(8,128)(2,1)} %all-gather.9.cloned.1.call-done), kind=kOutput, calls=%fused_computation.4 | convolution fusion | flops 2952790016 | bytes 10747904 | tf_op jit(solution)/shard_map/dot_general | solution.py:58
  169.3 17.0 %all-gather.11.cloned.1.call-done = bf16[1408,2048]{1,0:T(8,128)(2,1)} async-done(((bf16[1408,256]{1,0:T(8,128)(2,1)}), bf16[1408,2048]{1,0:T(8,128)(2,1)}) %all-gather.11.cloned.1.call-update) | async-done | bytes 5767184 | tf_op jit(solution)/shard_map/all_gather | solution.py:52
  186.3 7.6 %fusion.3 = f32[512,1408]{1,0:T(8,128)} fusion(bf16[512,2048]{1,0:T(8,128)(2,1)S(1)} %copy-done.1, bf16[1408,2048]{1,0:T(8,128)(2,1)} %all-gather.11.cloned.1.call-done), kind=kOutput, calls=%fused_computation.25 | convolution fusion | flops 2952790016 | bytes 10747904 | tf_op jit(solution)/shard_map/dot_general | solution.py:57
  193.9 14.6 %all-gather.5.cloned.1.call-done = bf16[512,2048]{1,0:T(8,128)(2,1)} async-done(((bf16[128,2048]{1,0:T(8,128)(2,1)}), bf16[512,2048]{1,0:T(8,128)(2,1)}) %all-gather.5.cloned.1.call-update) | async-done | bytes 2097168 | tf_op jit(solution)/shard_map/all_gather | solution.py:49
  208.5 95.1 %all-gather.7.cloned.1.call-done = bf16[1408,2048]{1,0:T(8,128)(2,1)} async-done(((bf16[1408,256]{1,0:T(8,128)(2,1)}), bf16[1408,2048]{1,0:T(8,128)(2,1)}) %all-gather.7.cloned.1.call-update) | async-done | bytes 5767184 | tf_op jit(solution)/shard_map/all_gather | solution.py:54
  303.6 9.1 %multiply_convert_fusion.4 = (bf16[512,1408]{1,0:T(8,128)(2,1)S(1)}, bf16[512,1408]{1,0:T(8,128)(2,1)S(1)}) fusion(f32[512,1408]{1,0:T(8,128)} %fusion.3, f32[512,1408]{1,0:T(8,128)} %convolution_bitcast_fusion, bf16[512,2048]{1,0:T(8,128)(2,1)} %all-gather.5.cloned.1.call-done, bf16[1408,2048]{1,0:T(8,128)(2,1)} %all-gather.7.cloned.1.call-done), kind=kOutput, calls=%fused_computation.6 | convolution fusion | flops 2962161664 | bytes 16515072 | tf_op jit(solution)/shard_map/dot_general | solution.py:59
  313.8 5.0 multiply_convert_fusion.2
  319.0 5.0 multiply_convert_fusion.1
  324.1 1.6 copy-done.2
  325.7 8.0 %multiply_convert_fusion = bf16[1408,2048]{1,0:T(8,128)(2,1)} fusion(bf16[512,2048]{1,0:T(8,128)(2,1)S(1)} %copy-done.2, f32[512,1408]{1,0:T(8,128)} %convolution_bitcast_fusion, f32[512,1408]{1,0:T(8,128)} %fusion.3), kind=kOutput, calls=%fused_computation | convolution fusion | flops 2962882560 | bytes 13631488 | tf_op jit(solution)/shard_map/dot_general | solution.py:77
  333.7 1.3 copy-done.4
  335.0 5.4 fusion.4
  340.4 7.4 %add_convert_fusion = bf16[512,2048]{1,0:T(8,128)(2,1)} fusion(f32[512,2048]{1,0:T(8,128)S(1)} %fusion.4, bf16[512,1408]{1,0:T(8,128)(2,1)S(1)} %get-tuple-element.16, bf16[1408,2048]{1,0:T(8,128)(2,1)} %constant_dynamic-update-slice_fusion), kind=kOutput, calls=%fused_computation.3 | convolution fusion | flops 2954887168 | bytes 13500416 | tf_op jit(solution)/shard_map/dot_general | solution.py:67
  347.9 80.2 %reduce-scatter.7.cloned.1.call-done = bf16[1408,256]{1,0:T(8,128)(2,1)} async-done(((bf16[1408,2048]{1,0:T(8,128)(2,1)}), bf16[1408,256]{1,0:T(8,128)(2,1)}) %reduce-scatter.7.cloned.1.call-update) | async-done | bytes 720912 | tf_op jit(solution)/shard_map/reduce_scatter | solution.py:79
  428.1 2.3 multiply_reduce_fusion.2
  430.5 111.6 %reduce-scatter.9.cloned.1.call-done = bf16[1408,256]{1,0:T(8,128)(2,1)} async-done(((bf16[1408,2048]{1,0:T(8,128)(2,1)}), bf16[1408,256]{1,0:T(8,128)(2,1)}) %reduce-scatter.9.cloned.1.call-update) | async-done | bytes 720912 | tf_op jit(solution)/shard_map/reduce_scatter | solution.py:82
  542.1 2.3 multiply_reduce_fusion.1
  544.4 111.7 %reduce-scatter.11.cloned.1.call-done = bf16[1408,256]{1,0:T(8,128)(2,1)} async-done(((bf16[1408,2048]{1,0:T(8,128)(2,1)}), bf16[1408,256]{1,0:T(8,128)(2,1)}) %reduce-scatter.11.cloned.1.call-update) | async-done | bytes 720912 | tf_op jit(solution)/shard_map/reduce_scatter | solution.py:85
  656.1 2.3 multiply_reduce_fusion
  658.5 35.5 %all-reduce = (f32[1408]{0:T(1024)S(1)}, f32[1408]{0:T(1024)S(1)}, f32[1408]{0:T(1024)S(1)}) all-reduce(f32[1408]{0:T(1024)S(1)} %get-tuple-element.14, f32[1408]{0:T(1024)S(1)} %get-tuple-element.12, f32[1408]{0:T(1024)S(1)} %get-tuple-element.10), channel_id=1, replica_groups=mesh['fs'=8,'tp'=4] {'fs'}, use_global_device_ids=true, to_apply=%region_5.6 | all-reduce | flops 4224 | bytes 33792 | tf_op jit(solution)/shard_map/psum | solution.py:89
  (39 shorter events, 13.9 us)
Async XLA Ops:
  7.2 153.7 %all-gather.9.cloned.1.call-start = ((), (), s32[]{:S(2)}) async-start(), calls=%async_computation.6 | async-start | bytes 2621440 | tf_op jit(solution)/shard_map/all_gather | solution.py:48
  7.9 178.4 %all-gather.11.cloned.1.call-start = ((), (), s32[]{:S(2)}) async-start(), calls=%async_computation.7 | async-start | bytes 6488064 | tf_op jit(solution)/shard_map/all_gather | solution.py:52
  8.7 199.9 %all-gather.5.cloned.1.call-start = ((), (), s32[]{:S(2)}) async-start(), calls=%async_computation.4 | async-start | bytes 2621440 | tf_op jit(solution)/shard_map/all_gather | solution.py:49
  9.4 294.2 %all-gather.7.cloned.1.call-start = ((), (), s32[]{:S(2)}) async-start(), calls=%async_computation.5 | async-start | bytes 6488064 | tf_op jit(solution)/shard_map/all_gather | solution.py:54
  10.0 418.2 %reduce-scatter.7.cloned.1.call-start = ((), (), s32[]{:S(2)}) async-start(), calls=%async_computation.9 | async-start | bytes 6488064 | tf_op jit(solution)/shard_map/reduce_scatter | solution.py:79
  10.0 34.2 %collective-permute-start = (bf16[1408,256]{1,0:T(8,128)(2,1)}, bf16[1408,256]{1,0:T(8,128)(2,1)S(1)}, u32[]{:S(2)}, u32[]{:S(2)}) collective-permute-start(bf16[1408,256]{1,0:T(8,128)(2,1)} %param.7), channel_id=1, source_target_pairs={{0,4},{4,8},{8,12},{12,16},{16,20},{20,24},{24,28},{28,0},{1,5},{5... | collective-permute-start | bytes 2162696 | tf_op jit(solution)/shard_map/ppermute | solution.py:25
  13.0 33.5 %collective-permute-start.1 = (bf16[1408,256]{1,0:T(8,128)(2,1)}, bf16[1408,256]{1,0:T(8,128)(2,1)S(1)}, u32[]{:S(2)}, u32[]{:S(2)}) collective-permute-start(bf16[1408,256]{1,0:T(8,128)(2,1)} %param.7), channel_id=1, source_target_pairs={{0,28},{4,0},{8,4},{12,8},{16,12},{20,16},{24,20},{28,24},{1,29},{... | collective-permute-start | bytes 2162696 | tf_op jit(solution)/shard_map/ppermute | solution.py:35
  44.2 40.0 %collective-permute-start.2 = (bf16[1408,256]{1,0:T(8,128)(2,1)S(1)}, bf16[1408,256]{1,0:T(8,128)(2,1)S(1)}, u32[]{:S(2)}, u32[]{:S(2)}) collective-permute-start(bf16[1408,256]{1,0:T(8,128)(2,1)S(1)} %collective-permute-done), channel_id=1, source_target_pairs={{0,4},{4,8},{8,12},{12,16},{16,20},{20,24},{24,28},{28,0},{1,5},{5... | collective-permute-start | bytes 2162696 | tf_op jit(solution)/shard_map/ppermute | solution.py:25
  46.6 6.3 copy-start
  46.6 42.1 %collective-permute-start.3 = (bf16[1408,256]{1,0:T(8,128)(2,1)S(1)}, bf16[1408,256]{1,0:T(8,128)(2,1)S(1)}, u32[]{:S(2)}, u32[]{:S(2)}) collective-permute-start(bf16[1408,256]{1,0:T(8,128)(2,1)S(1)} %collective-permute-done.1), channel_id=1, source_target_pairs={{0,28},{4,0},{8,4},{12,8},{16,12},{20,16},{24,20},{28,24},{1,29},{... | collective-permute-start | bytes 2162696 | tf_op jit(solution)/shard_map/ppermute | solution.py:35
  84.2 41.6 %collective-permute-start.4 = (bf16[1408,256]{1,0:T(8,128)(2,1)S(1)}, bf16[1408,256]{1,0:T(8,128)(2,1)S(1)}, u32[]{:S(2)}, u32[]{:S(2)}) collective-permute-start(bf16[1408,256]{1,0:T(8,128)(2,1)S(1)} %collective-permute-done.2), channel_id=1, source_target_pairs={{0,4},{4,8},{8,12},{12,16},{16,20},{20,24},{24,28},{28,0},{1,5},{5... | collective-permute-start | bytes 2162696 | tf_op jit(solution)/shard_map/ppermute | solution.py:25
  88.6 42.4 %collective-permute-start.5 = (bf16[1408,256]{1,0:T(8,128)(2,1)S(1)}, bf16[1408,256]{1,0:T(8,128)(2,1)S(1)}, u32[]{:S(2)}, u32[]{:S(2)}) collective-permute-start(bf16[1408,256]{1,0:T(8,128)(2,1)S(1)} %collective-permute-done.3), channel_id=1, source_target_pairs={{0,28},{4,0},{8,4},{12,8},{16,12},{20,16},{24,20},{28,24},{1,29},{... | collective-permute-start | bytes 2162696 | tf_op jit(solution)/shard_map/ppermute | solution.py:35
  125.9 34.0 %collective-permute-start.6 = (bf16[1408,256]{1,0:T(8,128)(2,1)S(1)}, bf16[1408,256]{1,0:T(8,128)(2,1)S(1)}, u32[]{:S(2)}, u32[]{:S(2)}) collective-permute-start(bf16[1408,256]{1,0:T(8,128)(2,1)S(1)} %collective-permute-done.4), channel_id=1, source_target_pairs={{0,4},{4,8},{8,12},{12,16},{16,20},{20,24},{24,28},{28,0},{1,5},{5... | collective-permute-start | bytes 2162696 | tf_op jit(solution)/shard_map/ppermute | solution.py:25
  160.8 25.5 %copy-start.1 = (bf16[512,2048]{1,0:T(8,128)(2,1)S(1)}, bf16[512,2048]{1,0:T(8,128)(2,1)}, u32[]{:S(2)}) copy-start(bf16[512,2048]{1,0:T(8,128)(2,1)} %all-gather.9.cloned.1.call-done) | copy-start | bytes 6291460
  312.7 1.1 copy-start.3
  318.8 223.3 %reduce-scatter.9.cloned.1.call-start = ((), (), s32[]{:S(2)}) async-start(), calls=%async_computation.10 | async-start | bytes 6488064 | tf_op jit(solution)/shard_map/reduce_scatter | solution.py:82
  324.0 1.7 copy-start.2
  324.0 332.1 %reduce-scatter.11.cloned.1.call-start = ((), (), s32[]{:S(2)}) async-start(), calls=%async_computation.11 | async-start | bytes 6488064 | tf_op jit(solution)/shard_map/reduce_scatter | solution.py:85
  333.7 1.4 copy-start.4
  333.7 361.5 %reduce-scatter.5.cloned.1.call-start = ((), (), s32[]{:S(2)}) async-start(), calls=%async_computation.8 | async-start | bytes 2621440 | tf_op jit(solution)/shard_map/reduce_scatter | solution.py:66
Sparse Core Ops, SparseCore 0:
  9.5 25.2 all-gather.8
  36.9 149.3 all-gather.10
  187.8 20.6 all-gather.4
  210.4 93.1 all-gather.6
  318.9 109.1 reduce-scatter.6
  431.6 110.3 reduce-scatter.8
  545.7 110.3 reduce-scatter.10
  659.2 30.5 reduce-scatter.4
